TPU v7x, 32 devices: a whole 2x2x4 slice. The times are simulated.
32 devices in a mesh: sp: 8 (over z, y), tp: 4 (over x, core).
Axes of the slice: x: 2, y: 2, z: 4, core: 2. Of those that a mesh axis runs over, the one named last changes fastest.
Arguments:
- prompt_input: bfloat16 [2304, 2048], P('sp'), may hold values from -6 to 6
- next_input: bfloat16 [2048], replicated, may hold values from -6 to 6
- norm_gain: float32 [2048], replicated, may hold values from 0.1 to 1.9
- w_key: bfloat16 [2048, 1024], P(None, 'tp'), may hold values from -0.125 to 0.125
- w_value: bfloat16 [2048, 1024], P(None, 'tp'), may hold values from -0.125 to 0.125
- w_query: bfloat16 [2048, 1024], P(None, 'tp'), may hold values from -0.125 to 0.125
- key_offset: float32 [2304, 8], P('sp', 'tp'), may hold values from -10 to 0, as said below
Outputs:
- key_cache: bfloat16 [8, 8, 36, 1024], P('sp', None, None, 'tp')
- value_cache: bfloat16 [8, 8, 36, 1024], P('sp', None, None, 'tp')
- reading: bfloat16 [1024], replicated
Inputs may be any that keep to these rules, and one draw needn't show every extreme that they name: `key_offset`: finite log-odds offsets, one per key and head.
All inputs are finite; a program needn't handle non-finite values.
Results may differ from a plain program's by a relative error of at most 0.011.
Values may be sent and summed in bfloat16 or wider, within the bound.
A program may use at most 64 MiB of HBM per device.

v0:
```python
import jax
import jax.numpy as jnp
from jax import lax
from jax.sharding import PartitionSpec as P

HEAD_DIM = 128


def norm_rows(row_block, gain_vec):
    wide_rows = row_block.astype(jnp.float32)
    inv_rms = lax.rsqrt(jnp.mean(wide_rows * wide_rows, axis=-1, keepdims=True) + 1e-06)
    return (wide_rows * inv_rms * gain_vec).astype(jnp.bfloat16)


def shards(prompt_input, next_input, norm_gain, w_key, w_value, w_query, key_offset):
    span_len = prompt_input.shape[0]
    head_width = w_key.shape[1]
    heads_here = head_width // HEAD_DIM
    score_scale = HEAD_DIM ** (-0.5)
    slots = lax.axis_size("sp")
    sub_len = span_len // slots
    normed = norm_rows(prompt_input, norm_gain)
    key_rows = jnp.dot(normed, w_key, preferred_element_type=jnp.float32).astype(jnp.bfloat16)
    value_rows = jnp.dot(normed, w_value, preferred_element_type=jnp.float32).astype(jnp.bfloat16)
    outgoing = jnp.stack([key_rows, value_rows]).reshape(2, slots, 1, sub_len, head_width)
    arrived = lax.all_to_all(outgoing, "sp", split_axis=1, concat_axis=2, tiled=True)
    key_cache = arrived[0]
    value_cache = arrived[1]
    new_query = jnp.dot(
        norm_rows(next_input[None, :], norm_gain), w_query, preferred_element_type=jnp.float32
    )
    new_query = new_query.astype(jnp.bfloat16).reshape(heads_here, HEAD_DIM)
    key_heads = key_rows.reshape(span_len, heads_here, HEAD_DIM)
    value_heads = value_rows.reshape(span_len, heads_here, HEAD_DIM)
    logits = (
        jnp.einsum("hd,shd->sh", new_query, key_heads, preferred_element_type=jnp.float32)
        * score_scale
        + key_offset
    )
    log_breaks = jax.nn.log_sigmoid(-logits)
    inner_sum = lax.cumsum(log_breaks, axis=0, reverse=True) - log_breaks
    block_totals = jnp.sum(log_breaks, axis=0)
    every_total = lax.all_gather(block_totals[None], "sp", axis=0, tiled=True)
    block_ids = lax.broadcasted_iota(jnp.int32, every_total.shape, 0)
    carried = jnp.sum(jnp.where(block_ids > lax.axis_index("sp"), every_total, 0.0), axis=0)
    weights = jnp.exp(jax.nn.log_sigmoid(logits) + inner_sum + carried[None, :])
    partial_value = jnp.einsum("sh,shd->hd", weights, value_heads.astype(jnp.float32))
    summed = lax.psum(partial_value, "sp")
    own_read = summed.reshape(head_width).astype(jnp.bfloat16)
    reading = lax.all_gather(own_read, "tp", axis=0, tiled=True)
    return (key_cache, value_cache, reading)


def solution(mesh):
    placed = (P("sp", None), P(), P(), P(None, "tp"), P(None, "tp"), P(None, "tp"), P("sp", "tp"))
    return jax.shard_map(
        shards,
        mesh=mesh,
        in_specs=placed,
        out_specs=(P("sp", None, None, "tp"), P("sp", None, None, "tp"), P()),
        check_vma=False,
    )
```

profile of v0, /device:TPU:0, one launch (start us, length us, event | category | flops | bytes accessed | tf_op | source)
XLA Modules:
  0.0 65.4 jit_solution(9334492287471043287)
XLA Ops:
  0.6 0.0 copy-start
  0.6 0.0 copy-start.1
  0.7 1.7 %fusion = f32[288]{0:T(512)S(1)} fusion(bf16[288,2048]{1,0:T(8,128)(2,1)} %param.7), kind=kLoop, calls=%fused_computation.2 | loop fusion | flops 1769184 | bytes 1180800 | tf_op jit(solution)/shard_map/reduce_sum | solution.py:11
  2.4 0.0 copy-done
  2.4 0.2 copy-done.1
  2.6 0.0 copy-start.5
  2.6 0.0 copy-start.6
  2.6 1.3 %convolution_convert_fusion = bf16[288,256]{1,0:T(8,128)(2,1)S(1)} fusion(bf16[2048,256]{1,0:T(8,128)(2,1)S(1)} %copy-done, bf16[288,2048]{1,0:T(8,128)(2,1)S(1)} %copy-done.1, f32[2048]{0:T(1024)} %param.9, f32[288]{0:T(512)S(1)} %add_rsqrt_fusion), kind=kOutput, calls=%fused_computation.5 | convolution fusion | flops 304422912 | bytes 2385024 | tf_op jit(solution)/shard_map/dot_general | solution.py:24
  3.9 0.0 copy-done.5
  3.9 0.0 copy-done.6
  3.9 0.5 convolution_convert_fusion.1
  4.5 0.0 copy-start.3
  4.5 0.0 copy-start.2
  4.6 0.0 copy-start.7
  4.6 0.0 copy-start.4
  4.6 1.0 %copy.17 = bf16[2,8,1,36,256]{4,0,3,2,1:T(2,128)(2,1)} copy(bf16[2,8,1,36,256]{4,3,1,2,0:T(8,128)(2,1)S(1)} %pad_maximum_fusion) | data formatting | bytes 589824 | tf_op jit(solution)/shard_map/stack | solution.py:25
  5.6 7.3 %all-to-all-start = ((bf16[2,8,1,36,256]{4,0,3,2,1:T(2,128)(2,1)}), bf16[2,8,1,36,256]{4,0,3,2,1:T(2,128)(2,1)S(1)}, u32[]{:S(2)}, u32[]{:S(2)}) async-start(bf16[2,8,1,36,256]{4,0,3,2,1:T(2,128)(2,1)} %copy.17), calls=%async_computation | async-start | bytes 589824 | tf_op jit(solution)/shard_map/all_to_all | solution.py:26
  13.0 0.0 copy-done.3
  13.0 0.6 fusion.11
  14.3 0.0 copy-done.2
  14.3 0.2 fusion.21
  14.5 0.1 fusion.8
  14.7 0.0 copy-done.7
  14.7 0.6 dynamic-slice
  16.0 0.0 copy-done.4
  16.0 0.1 fusion.19
  16.1 0.1 negate_dynamic-update-slice_fusion
  16.2 21.8 %all-reduce.1 = f32[16]{0:T(128)S(1)} all-reduce(f32[16]{0:T(128)S(1)} %negate_dynamic-update-slice_fusion), channel_id=2, replica_groups=mesh['sp'=8,'tp'=4] {'sp'}, use_global_device_ids=true, to_apply=%add.1 | all-reduce | flops 16 | bytes 128
  38.1 2.5 %reduce-window.6 = f32[2,3,128]{2,1,0:T(4,128)S(1)} reduce-window(f32[2,3,128]{2,1,0:T(4,128)S(1)} %reshape.81, f32[]{:T(128)} %constant.20.clone.1), window={size=1x1x128 pad=0_0x0_0x0_127}, to_apply=%region_2.3 | reduce-window | flops 97536 | bytes 6148 | tf_op jit(solution)/shard_map/reduce-window
  40.6 0.1 slice_reduce_fusion
  40.7 0.2 reduce-window.9
  40.9 0.1 slice.21
  40.9 0.1 add_bitcast_fusion
  41.0 0.1 reshape.84
  41.1 0.1 select_reduce_fusion
  41.2 0.1 exponential_bitcast_fusion
  41.3 0.1 fusion.5
  41.4 17.1 %psum.7 = bf16[2,128]{1,0:T(2,128)(2,1)S(1)} all-reduce(f32[2,128]{1,0:T(2,128)S(1)} %bitcast.64), channel_id=1, replica_groups=mesh['sp'=8,'tp'=4] {'sp'}, use_global_device_ids=true, to_apply=%region_6.7 | all-reduce | flops 256 | bytes 1536 | tf_op jit(solution)/shard_map/psum | solution.py:48
  58.6 5.1 %all-gather.1 = bf16[4,1,256]{2,1,0:T(2,128)(2,1)S(1)} all-gather(bf16[1,1,256]{2,1,0:T(2,128)(2,1)S(1)} %reshape.88), channel_id=1, replica_groups=mesh['sp'=8,'tp'=4] {'tp'}, dimensions={0}, use_global_device_ids=true | all-gather | bytes 2560 | tf_op jit(solution)/shard_map/all_gather | solution.py:50
  63.6 0.6 copy.31
  64.2 0.0 all-to-all-done
  64.2 0.4 fusion.20
  64.6 0.8 %copy_bitcast_fusion = (bf16[1,8,36,256]{3,1,2,0:T(8,128)(2,1)}, bf16[1,8,36,256]{3,1,2,0:T(8,128)(2,1)}) fusion(bf16[1,8,1,36,256]{4,0,3,2,1:T(2,128)(2,1)S(1)} %get-tuple-element.11, bf16[1,8,1,36,256]{4,0,3,2,1:T(2,128)(2,1)S(1)} %get-tuple-element.12), kind=kLoop, calls=%fused_computation.14 | loop fusion | bytes 589824 | tf_op jit(solution)/shard_map/squeeze | solution.py:28
  (15 shorter events, 0.2 us)
Async XLA Ops:
  0.6 1.8 %copy-start = (bf16[2048,256]{1,0:T(8,128)(2,1)S(1)}, bf16[2048,256]{1,0:T(8,128)(2,1)}, u32[]{:S(2)}) copy-start(bf16[2048,256]{1,0:T(8,128)(2,1)} %param.11) | copy-start | bytes 3145732
  0.6 1.9 %copy-start.1 = (bf16[288,2048]{1,0:T(8,128)(2,1)S(1)}, bf16[288,2048]{1,0:T(8,128)(2,1)}, u32[]{:S(2)}) copy-start(bf16[288,2048]{1,0:T(8,128)(2,1)} %param.7) | copy-start | bytes 3538948
  2.6 1.3 %copy-start.5 = (f32[2048]{0:T(1024)S(1)}, f32[2048]{0:T(1024)}, u32[]{:S(2)}) copy-start(f32[2048]{0:T(1024)} %param.9) | copy-start | bytes 24580
  2.6 1.3 %copy-start.6 = (bf16[2048,256]{1,0:T(8,128)(2,1)S(1)}, bf16[2048,256]{1,0:T(8,128)(2,1)}, u32[]{:S(2)}) copy-start(bf16[2048,256]{1,0:T(8,128)(2,1)} %param.10) | copy-start | bytes 3145732
  4.5 8.5 %copy-start.3 = (bf16[2048]{0:T(1024)(128)(2,1)S(1)}, bf16[2048]{0:T(1024)(128)(2,1)}, u32[]{:S(2)}) copy-start(bf16[2048]{0:T(1024)(128)(2,1)} %param.8) | copy-start | bytes 12292
  4.5 9.8 %copy-start.2 = (bf16[2048,256]{1,0:T(8,128)(2,1)S(1)}, bf16[2048,256]{1,0:T(8,128)(2,1)}, u32[]{:S(2)}) copy-start(bf16[2048,256]{1,0:T(8,128)(2,1)} %param.12) | copy-start | bytes 3145732
  4.6 10.1 %copy-start.7 = (u32[32]{0:T(128)S(1)}, u32[32]{0:T(128)}, u32[]{:S(2)}) copy-start(u32[32]{0:T(128)} %constant.31) | copy-start | bytes 388
  4.6 11.3 %copy-start.4 = (f32[288,2]{0,1:T(2,128)S(1)}, f32[288,2]{0,1:T(2,128)}, u32[]{:S(2)}) copy-start(f32[288,2]{0,1:T(2,128)} %param.13) | copy-start | bytes 6916
  5.6 58.6 %all-to-all-start = ((bf16[2,8,1,36,256]{4,0,3,2,1:T(2,128)(2,1)}), bf16[2,8,1,36,256]{4,0,3,2,1:T(2,128)(2,1)S(1)}, u32[]{:S(2)}, u32[]{:S(2)}) async-start(bf16[2,8,1,36,256]{4,0,3,2,1:T(2,128)(2,1)} %copy.17), calls=%async_computation | async-start | bytes 589824 | tf_op jit(solution)/shard_map/all_to_all | solution.py:26
where the time goes:
time: 65.7 us; the launch traced here: 65.4 us
  blocking collectives  44 us (67%)
  starting transfers between devices  7.31 us (11%)
  other arithmetic  5.61 us (9%)
  local copies, waits for them, and re-layouts  3.98 us (6%)
  matrix products  2.36 us (4%)
  between operations  2.15 us (3%)
    unnamed x1, blocking collectives  21.8 us
    psum x1, blocking collectives, shards(): summed = lax.psum(partial_value, 'sp')  17.1 us
    all_to_all x1, starting transfers between devices, shards(): lax.all_to_all(outgoing, 'sp', split_axis=1, concat_axis=2, tiled=True)  7.31 us
    all_gather x1, blocking collectives, shards(): reading = lax.all_gather(own_read, 'tp', axis=0, tiled=True)  5.05 us
    another operation x2, other arithmetic  2.71 us
    reduce_sum x2, other arithmetic, norm_rows(): jnp.mean(wide_rows * wide_rows, axis=-1, keepdims=True) + 1e-06  2.34 us
    unnamed x21, local copies, waits for them, and re-layouts  1.43 us
  transfers between devices with their start and end apart: 1, of which 0 were waited for; matrix products, arithmetic and copies ran while one was open for 9% of the time, Pallas kernels for 0%

commit v1 on v0

--- a/solution.py
+++ b/solution.py
@@ -23,7 +23,10 @@
     key_rows = jnp.dot(normed, w_key, preferred_element_type=jnp.float32).astype(jnp.bfloat16)
     value_rows = jnp.dot(normed, w_value, preferred_element_type=jnp.float32).astype(jnp.bfloat16)
     outgoing = jnp.stack([key_rows, value_rows]).reshape(2, slots, 1, sub_len, head_width)
-    arrived = lax.all_to_all(outgoing, "sp", split_axis=1, concat_axis=2, tiled=True)
+    arrived = jnp.concatenate(
+        lax.all_to_all(jnp.stack(jnp.split(outgoing, lax.axis_size("sp"), axis=1)), "sp", 0, 0),
+        axis=2,
+    )
     key_cache = arrived[0]
     value_cache = arrived[1]
     new_query = jnp.dot(

time: 65.7 us -> 65.4 us (level)
    another operation x3, local copies, waits for them, and re-layouts: 1.07 us -> 0.08 us  [shards(): jnp.stack([key_rows, value_rows]).reshape(2, slots, 1, sub_len, head_width)]
    another operation x1 -> x3, local copies, waits for them, and re-layouts: 0.07 us -> 1.01 us  [the longest x2 0.94 us: shards(): jnp.stack(jnp.split(outgoing, lax.axis_size('sp'), axis=1))]
    unnamed x21 -> x29, local copies, waits for them, and re-layouts: 1.43 us -> 1.47 us
    another operation x3 -> x2, other arithmetic: 2.74 us -> 2.71 us
where the time goes in v1:
time: 65.4 us; the launch traced here: 65 us
  blocking collectives  44 us (67%)
  starting transfers between devices  7.31 us (11%)
  other arithmetic  5.57 us (9%)
  local copies, waits for them, and re-layouts  3.55 us (5%)
  matrix products  2.35 us (4%)
  between operations  2.22 us (3%)
    unnamed x1, blocking collectives  21.8 us
    psum x1, blocking collectives, shards(): summed = lax.psum(partial_value, 'sp')  17.1 us
    all_to_all x1, starting transfers between devices, shards(): lax.all_to_all(jnp.stack(jnp.split(outgoing, lax.axis_size('sp'), axis=1)...  7.31 us
    all_gather x1, blocking collectives, shards(): reading = lax.all_gather(own_read, 'tp', axis=0, tiled=True)  5.05 us
    another operation x2, other arithmetic  2.71 us
    reduce_sum x2, other arithmetic, norm_rows(): jnp.mean(wide_rows * wide_rows, axis=-1, keepdims=True) + 1e-06  2.34 us
    unnamed x29, local copies, waits for them, and re-layouts  1.47 us
  transfers between devices with their start and end apart: 1, of which 0 were waited for; matrix products, arithmetic and copies ran while one was open for 9% of the time, Pallas kernels for 0%

profile of v1, /device:TPU:0, one launch (start us, length us, event | category | flops | bytes accessed | tf_op | source)
XLA Modules:
  0.0 65.0 jit_solution(1854407238710494728)
XLA Ops:
  0.6 0.0 copy-start
  0.6 0.0 copy-start.1
  0.7 1.7 %fusion = f32[288]{0:T(512)S(1)} fusion(bf16[288,2048]{1,0:T(8,128)(2,1)} %param.7), kind=kLoop, calls=%fused_computation.2 | loop fusion | flops 1769184 | bytes 1180800 | tf_op jit(solution)/shard_map/reduce_sum | solution.py:11
  2.4 0.0 copy-done
  2.4 0.2 copy-done.1
  2.6 0.0 copy-start.5
  2.6 0.0 copy-start.6
  2.6 1.3 %convolution_convert_fusion = bf16[288,256]{1,0:T(8,128)(2,1)S(1)} fusion(bf16[2048,256]{1,0:T(8,128)(2,1)S(1)} %copy-done, bf16[288,2048]{1,0:T(8,128)(2,1)S(1)} %copy-done.1, f32[2048]{0:T(1024)} %param.9, f32[288]{0:T(512)S(1)} %add_rsqrt_fusion), kind=kOutput, calls=%fused_computation.5 | convolution fusion | flops 304422912 | bytes 2385024 | tf_op jit(solution)/shard_map/dot_general | solution.py:24
  3.9 0.0 copy-done.5
  3.9 0.0 copy-done.6
  3.9 0.5 convolution_convert_fusion.1
  4.6 0.0 copy-start.3
  4.6 0.0 copy-start.2
  4.7 0.0 copy-start.7
  4.7 0.0 copy-start.4
  4.7 0.9 %copy.48 = bf16[8,2,1,1,36,256]{5,1,4,3,2,0:T(2,128)(2,1)} copy(bf16[8,2,1,1,36,256]{5,4,1,3,2,0:T(8,128)(2,1)S(1)} %fusion.11) | data formatting | bytes 589824 | tf_op jit(solution)/shard_map/stack | solution.py:27
  5.7 7.3 %all-to-all-start = ((bf16[8,2,1,1,36,256]{5,1,4,3,2,0:T(2,128)(2,1)}), bf16[8,2,1,1,36,256]{5,1,4,3,2,0:T(2,128)(2,1)S(1)}, u32[]{:S(2)}, u32[]{:S(2)}) async-start(bf16[8,2,1,1,36,256]{5,1,4,3,2,0:T(2,128)(2,1)} %copy.48), calls=%async_computation | async-start | bytes 589824 | tf_op jit(solution)/shard_map/all_to_all | solution.py:27
  13.0 0.0 copy-done.3
  13.0 0.6 fusion.19
  14.3 0.0 copy-done.2
  14.3 0.2 fusion.28
  14.6 0.1 fusion.8
  14.7 0.0 copy-done.7
  14.7 0.6 dynamic-slice
  16.0 0.0 copy-done.4
  16.0 0.1 fusion.27
  16.1 0.1 negate_dynamic-update-slice_fusion
  16.2 21.8 %all-reduce.1 = f32[16]{0:T(128)S(1)} all-reduce(f32[16]{0:T(128)S(1)} %negate_dynamic-update-slice_fusion), channel_id=2, replica_groups=mesh['sp'=8,'tp'=4] {'sp'}, use_global_device_ids=true, to_apply=%add.1 | all-reduce | flops 16 | bytes 128
  38.1 2.5 %reduce-window.6 = f32[2,3,128]{2,1,0:T(4,128)S(1)} reduce-window(f32[2,3,128]{2,1,0:T(4,128)S(1)} %reshape.81, f32[]{:T(128)} %constant.20.clone.1), window={size=1x1x128 pad=0_0x0_0x0_127}, to_apply=%region_2.3 | reduce-window | flops 97536 | bytes 6148 | tf_op jit(solution)/shard_map/reduce-window
  40.6 0.1 slice_reduce_fusion
  40.7 0.2 reduce-window.9
  40.9 0.1 slice.20
  41.0 0.1 add_bitcast_fusion
  41.0 0.1 reshape.84
  41.1 0.1 select_reduce_fusion
  41.2 0.1 exponential_bitcast_fusion
  41.3 0.1 fusion.5
  41.4 17.1 %psum.7 = bf16[2,128]{1,0:T(2,128)(2,1)S(1)} all-reduce(f32[2,128]{1,0:T(2,128)S(1)} %bitcast.112), channel_id=1, replica_groups=mesh['sp'=8,'tp'=4] {'sp'}, use_global_device_ids=true, to_apply=%region_6.7 | all-reduce | flops 256 | bytes 1536 | tf_op jit(solution)/shard_map/psum | solution.py:51
  58.6 5.1 %all-gather.1 = bf16[4,1,256]{2,1,0:T(2,128)(2,1)S(1)} all-gather(bf16[1,1,256]{2,1,0:T(2,128)(2,1)S(1)} %reshape.88), channel_id=1, replica_groups=mesh['sp'=8,'tp'=4] {'tp'}, dimensions={0}, use_global_device_ids=true | all-gather | bytes 2560 | tf_op jit(solution)/shard_map/all_gather | solution.py:53
  63.7 0.6 copy.66
  64.2 0.0 all-to-all-done
  64.2 0.1 copy.87
  64.3 0.7 %slice_bitcast_fusion = (bf16[1,8,36,256]{3,1,2,0:T(8,128)(2,1)}, bf16[1,8,36,256]{3,1,2,0:T(8,128)(2,1)}) fusion(bf16[2,1,8,1,36,256]{5,2,4,3,1,0:T(8,128)(2,1)S(1)} %bitcast.107), kind=kLoop, calls=%fused_computation.14 | loop fusion | bytes 589824 | tf_op jit(solution)/shard_map/squeeze | solution.py:31
  (24 shorter events, 0.2 us)
Async XLA Ops:
  0.6 1.8 %copy-start = (bf16[2048,256]{1,0:T(8,128)(2,1)S(1)}, bf16[2048,256]{1,0:T(8,128)(2,1)}, u32[]{:S(2)}) copy-start(bf16[2048,256]{1,0:T(8,128)(2,1)} %param.11) | copy-start | bytes 3145732
  0.6 1.9 %copy-start.1 = (bf16[288,2048]{1,0:T(8,128)(2,1)S(1)}, bf16[288,2048]{1,0:T(8,128)(2,1)}, u32[]{:S(2)}) copy-start(bf16[288,2048]{1,0:T(8,128)(2,1)} %param.7) | copy-start | bytes 3538948
  2.6 1.3 %copy-start.5 = (f32[2048]{0:T(1024)S(1)}, f32[2048]{0:T(1024)}, u32[]{:S(2)}) copy-start(f32[2048]{0:T(1024)} %param.9) | copy-start | bytes 24580
  2.6 1.3 %copy-start.6 = (bf16[2048,256]{1,0:T(8,128)(2,1)S(1)}, bf16[2048,256]{1,0:T(8,128)(2,1)}, u32[]{:S(2)}) copy-start(bf16[2048,256]{1,0:T(8,128)(2,1)} %param.10) | copy-start | bytes 3145732
  4.6 8.4 %copy-start.3 = (bf16[2048]{0:T(1024)(128)(2,1)S(1)}, bf16[2048]{0:T(1024)(128)(2,1)}, u32[]{:S(2)}) copy-start(bf16[2048]{0:T(1024)(128)(2,1)} %param.8) | copy-start | bytes 12292
  4.6 9.7 %copy-start.2 = (bf16[2048,256]{1,0:T(8,128)(2,1)S(1)}, bf16[2048,256]{1,0:T(8,128)(2,1)}, u32[]{:S(2)}) copy-start(bf16[2048,256]{1,0:T(8,128)(2,1)} %param.12) | copy-start | bytes 3145732
  4.7 10.0 %copy-start.7 = (u32[32]{0:T(128)S(1)}, u32[32]{0:T(128)}, u32[]{:S(2)}) copy-start(u32[32]{0:T(128)} %constant.31) | copy-start | bytes 388
  4.7 11.3 %copy-start.4 = (f32[288,2]{0,1:T(2,128)S(1)}, f32[288,2]{0,1:T(2,128)}, u32[]{:S(2)}) copy-start(f32[288,2]{0,1:T(2,128)} %param.13) | copy-start | bytes 6916
  5.7 58.6 %all-to-all-start = ((bf16[8,2,1,1,36,256]{5,1,4,3,2,0:T(2,128)(2,1)}), bf16[8,2,1,1,36,256]{5,1,4,3,2,0:T(2,128)(2,1)S(1)}, u32[]{:S(2)}, u32[]{:S(2)}) async-start(bf16[8,2,1,1,36,256]{5,1,4,3,2,0:T(2,128)(2,1)} %copy.48), calls=%async_computation | async-start | bytes 589824 | tf_op jit(solution)/shard_map/all_to_all | solution.py:27
